TPU v7x, 32 devices: a whole 2x2x4 slice. The times are simulated.
32 devices in a mesh: dp: 4 (over y, x), kv: 4 (over z), tp: 2 (over core).
Axes of the slice: x: 2, y: 2, z: 4, core: 2. Of those that a mesh axis runs over, the one named last changes fastest.
Arguments:
- layer_input: bfloat16 [128, 4096], P('dp', ('kv', 'tp')), parts along dimension 0, may hold values from -22 to 22
- gate_weight: bfloat16 [4096, 2048], P(('kv', 'tp')), may hold values from -0.09375 to 0.09375
- value_weight: bfloat16 [4096, 2048], P(('kv', 'tp')), may hold values from -0.09375 to 0.09375
- write_weight: bfloat16 [4096, 256], P(('kv', 'tp')), may hold values from -0.09375 to 0.09375
- read_weight: bfloat16 [4096, 256], P(('kv', 'tp')), may hold values from -0.09375 to 0.09375
- step_weight: bfloat16 [4096, 32], P(('kv', 'tp')), may hold values from -0.09375 to 0.09375
- value_taps: bfloat16 [4, 2048], replicated, may hold values from -3 to 3
- write_taps: bfloat16 [4, 256], replicated, may hold values from -3 to 3
- read_taps: bfloat16 [4, 256], replicated, may hold values from -3 to 3
- past_values: bfloat16 [128, 3, 2048], P(('dp', 'kv', 'tp')), parts along dimension 0, may hold values from -6 to 6
- past_writes: bfloat16 [128, 3, 256], P(('dp', 'kv', 'tp')), parts along dimension 0, may hold values from -6 to 6
- past_reads: bfloat16 [128, 3, 256], P(('dp', 'kv', 'tp')), parts along dimension 0, may hold values from -6 to 6
- step_bias: float32 [32], replicated, may hold values from -4 to -1
- decay_log: float32 [32], replicated, may hold values from 0 to 2.77
- skip_scale: float32 [32], replicated, may hold values from 0.5 to 2
- state_past: float32 [128, 32, 64, 128], P(('dp', 'kv', 'tp')), parts along dimension 0, may hold values from -3 to 3
- mixer_gain: float32 [2048], replicated, may hold values from 0.1 to 1.9
- out_weight: bfloat16 [2048, 4096], P(None, ('kv', 'tp')), may hold values from -0.125 to 0.125
- norm1_gain: float32 [4096], replicated, may hold values from 0.24 to 3.7
- up_weight: bfloat16 [4096, 16384], P(None, ('kv', 'tp')), may hold values from -0.09375 to 0.09375
- down_weight: bfloat16 [16384, 4096], P(('kv', 'tp')), may hold values from -0.0625 to 0.0625
- norm2_gain: float32 [4096], replicated, may hold values from 0.1 to 1.9
Outputs:
- layer_output: bfloat16 [128, 4096], P('dp', ('kv', 'tp')), parts along dimension 0
- state_next: float32 [128, 32, 64, 128], P(('dp', 'kv', 'tp')), parts along dimension 0
There are 4 independent parts, one for each index of `dp`. A program takes and returns all parts, laid end to end along the dimension named above; an argument that names none is the same for every part. Nothing has to cross between parts.
All inputs are finite; a program needn't handle non-finite values.
Results may differ from a plain program's by a relative error of at most 0.012.
Values may be sent and summed in bfloat16 or wider, within the bound.
A program may use at most 128 MiB of HBM per device.

v0:
```python
import jax
import jax.numpy as jnp
from jax import lax
from jax.sharding import PartitionSpec as P

HEADS = 32
HEAD_DIM = 64
STATE_DIM = 128
GROUPS = 2


RESIDUAL_SCALE = 2.0**0.25
NORM_EPSILON = 1e-05
MIXER_EPSILON = 1e-06


def conv_silu(current, earlier, kernel):
    stacked = jnp.concatenate([earlier, current[:, None, :]], 1).astype(jnp.float32)
    return jax.nn.silu(jnp.sum(stacked * kernel.astype(jnp.float32)[None], 1))


def mixer_step(
    gate,
    values,
    writes,
    reads,
    steps,
    value_taps,
    write_taps,
    read_taps,
    past_values,
    past_writes,
    past_reads,
    step_bias,
    decay_log,
    skip_scale,
    state_past,
    mixer_gain,
):
    seq_count = gate.shape[0]
    values_act = conv_silu(values, past_values, value_taps).reshape(seq_count, HEADS, HEAD_DIM)
    writes_act = conv_silu(writes, past_writes, write_taps).reshape(seq_count, GROUPS, STATE_DIM)
    reads_act = conv_silu(reads, past_reads, read_taps).reshape(seq_count, GROUPS, STATE_DIM)
    per_group = HEADS // GROUPS
    writes_head = jnp.repeat(writes_act, per_group, axis=1)
    reads_head = jnp.repeat(reads_act, per_group, axis=1)
    step_size = jax.nn.softplus(steps.astype(jnp.float32) + step_bias)
    decays = jnp.exp(-step_size * jnp.exp(decay_log))
    state_next = (
        decays[:, :, None, None] * state_past
        + (step_size[:, :, None] * values_act)[:, :, :, None] * writes_head[:, :, None, :]
    )
    readout = jnp.einsum("shpn,shn->shp", state_next, reads_head, precision=lax.Precision.HIGHEST)
    readout = readout + skip_scale[None, :, None] * values_act
    gated = readout.reshape(seq_count, HEADS * HEAD_DIM) * jax.nn.silu(gate.astype(jnp.float32))
    grouped = gated.reshape(seq_count, GROUPS, -1)
    grouped = grouped * lax.rsqrt(jnp.mean(jnp.square(grouped), -1, keepdims=True) + MIXER_EPSILON)
    mixed = (grouped.reshape(seq_count, -1) * mixer_gain).astype(jnp.bfloat16)
    return (mixed, state_next)


def layer_norm(rows, gain):
    average = jnp.mean(rows, -1, keepdims=True)
    variance = jnp.mean(jnp.square(rows - average), -1, keepdims=True)
    return (rows - average) * lax.rsqrt(variance + NORM_EPSILON) * gain


def on_device(
    layer_input,
    gate_weight,
    value_weight,
    write_weight,
    read_weight,
    step_weight,
    value_taps,
    write_taps,
    read_taps,
    past_values,
    past_writes,
    past_reads,
    step_bias,
    decay_log,
    skip_scale,
    state_past,
    mixer_gain,
    out_weight,
    norm1_gain,
    up_weight,
    down_weight,
    norm2_gain,
):
    seqs_here = state_past.shape[0]
    device_slot = lax.axis_index(("kv", "tp"))
    weights = (gate_weight, value_weight, write_weight, read_weight, step_weight)

    def input_terms():
        pieces = [
            jnp.dot(layer_input, weight, preferred_element_type=jnp.float32) for weight in weights
        ]
        return jnp.concatenate(pieces, 1)

    projected = lax.psum_scatter(
        input_terms(), ("kv", "tp"), scatter_dimension=0, tiled=True
    ).astype(jnp.bfloat16)
    bounds = [0]
    for weight in weights:
        bounds.append(bounds[-1] + weight.shape[1])
    gate, values, writes, reads, steps = [
        projected[:, bounds[index] : bounds[index + 1]] for index in range(5)
    ]
    mixed, state_next = mixer_step(
        gate,
        values,
        writes,
        reads,
        steps,
        value_taps,
        write_taps,
        read_taps,
        past_values,
        past_writes,
        past_reads,
        step_bias,
        decay_log,
        skip_scale,
        state_past,
        mixer_gain,
    )
    mix_out = jnp.dot(
        lax.all_gather(mixed, ("kv", "tp"), axis=0, tiled=True),
        out_weight,
        preferred_element_type=jnp.float32,
    ).astype(jnp.bfloat16)
    residual = RESIDUAL_SCALE * layer_input.astype(jnp.float32) + mix_out.astype(jnp.float32)
    whole_residual = lax.all_gather(residual, ("kv", "tp"), axis=1, tiled=True)
    normed_all = layer_norm(whole_residual, norm1_gain).astype(jnp.bfloat16)
    hidden = jnp.square(
        jax.nn.relu(jnp.dot(normed_all, up_weight, preferred_element_type=jnp.float32))
    ).astype(jnp.bfloat16)
    channel = lax.psum_scatter(
        jnp.dot(hidden, down_weight, preferred_element_type=jnp.float32),
        ("kv", "tp"),
        scatter_dimension=0,
        tiled=True,
    ).astype(jnp.bfloat16)
    normed_rows = lax.dynamic_slice_in_dim(normed_all, device_slot * seqs_here, seqs_here, 0)
    second = RESIDUAL_SCALE * normed_rows.astype(jnp.float32) + channel.astype(jnp.float32)
    finished = layer_norm(second, norm2_gain).astype(jnp.bfloat16)
    result = lax.all_to_all(finished, ("kv", "tp"), split_axis=1, concat_axis=0, tiled=True)
    return (result, state_next)


def solution(mesh):
    placed = (
        P("dp", ("kv", "tp")),
        P(("kv", "tp"), None),
        P(("kv", "tp"), None),
        P(("kv", "tp"), None),
        P(("kv", "tp"), None),
        P(("kv", "tp"), None),
        P(),
        P(),
        P(),
        P(("dp", "kv", "tp"), None, None),
        P(("dp", "kv", "tp"), None, None),
        P(("dp", "kv", "tp"), None, None),
        P(),
        P(),
        P(),
        P(("dp", "kv", "tp"), None, None, None),
        P(),
        P(None, ("kv", "tp")),
        P(),
        P(None, ("kv", "tp")),
        P(("kv", "tp"), None),
        P(),
    )
    return jax.shard_map(
        on_device,
        mesh=mesh,
        in_specs=placed,
        out_specs=(P("dp", ("kv", "tp")), P(("dp", "kv", "tp"), None, None, None)),
        check_vma=False,
    )
```

profile of v0, /device:TPU:0, one launch (start us, length us, event | category | flops | bytes accessed | tf_op | source)
XLA Modules:
  0.0 145.4 jit_solution(11964027075452254944)
XLA Ops:
  0.6 0.0 copy-start
  0.7 0.0 copy-start.18
  0.7 0.0 copy-start.2
  0.7 0.0 copy-start.3
  0.7 0.0 copy-start.4
  0.7 0.0 copy-start.6
  0.7 0.0 copy-start.13
  0.7 0.0 copy-start.14
  0.7 0.0 copy-start.12
  0.7 0.0 copy-start.11
  0.7 0.0 copy-start.7
  0.8 0.0 copy-start.5
  0.8 0.0 copy-start.17
  0.8 0.0 copy-start.16
  0.8 1.6 %copy-done = bf16[512,2048]{1,0:T(8,128)(2,1)S(1)} copy-done((bf16[512,2048]{1,0:T(8,128)(2,1)S(1)}, bf16[512,2048]{1,0:T(8,128)(2,1)}, u32[]{:S(2)}) %copy-start) | copy-done | bytes 2097176
  2.4 1.2 convolution_dynamic-update-slice_fusion.1
  3.6 2.1 %convolution_dynamic-update-slice_fusion = f32[32,4640]{1,0:T(8,128)S(1)} fusion(f32[32,4640]{1,0:T(8,128)S(1)} %convolution_dynamic-update-slice_fusion.1, bf16[32,512]{1,0:T(8,128)(2,1)} %param.22, bf16[512,2048]{1,0:T(8,128)(2,1)} %param.24), kind=kOutput, calls=%fused_computation.1 | convolution fusion | flops 67108864 | bytes 2392064 | tf_op jit(solution)/shard_map/dot_general | solution.py:98
  5.7 0.0 copy-done.2
  5.7 0.0 copy-done.3
  5.7 0.1 convolution_dynamic-update-slice_fusion.3
  5.9 0.0 copy-done.4
  5.9 0.1 convolution_dynamic-update-slice_fusion.2
  6.1 0.0 copy-done.6
  6.1 0.1 convolution_dynamic-update-slice_fusion.4
  6.2 37.5 %all-reduce.4 = bf16[32,4640]{1,0:T(8,128)(2,1)S(1)} all-reduce(f32[32,4640]{1,0:T(8,128)S(1)} %convolution_dynamic-update-slice_fusion.4), channel_id=2, replica_groups=mesh['dp'=4,'kv'=4,'tp'=2] {'kv','tp'}, use_global_device_ids=true, to_apply=%region_0.0.clone | all-reduce | flops 148480 | bytes 890880
  43.7 0.0 copy-done.18
  43.8 0.6 dynamic-slice
  45.1 0.0 copy-done.13
  45.1 0.0 copy-done.14
  45.1 0.0 copy-done.12
  45.1 0.0 copy-done.11
  45.2 0.0 copy-done.7
  45.2 0.0 copy-done.5
  45.2 0.1 multiply_reduce_fusion.1
  45.3 0.1 reduce_sum.79
  45.4 0.0 copy-done.17
  45.4 0.0 copy-done.16
  45.5 0.1 broadcast_multiply_fusion
  45.6 3.7 %multiply_add_fusion = f32[4,32,64,128]{3,2,1,0:T(8,128)S(1)} fusion(f32[4,32,64,128]{3,2,1,0:T(8,128)} %param.37, f32[4,32,128]{2,1,0:T(8,128)S(1)} %bitcast.40, f32[4,32,64]{2,1,0:T(8,128)S(1)} %broadcast_multiply_fusion, f32[4,32]{1,0:T(4,128)S(1)} %get-tuple-element.4), kind=kLoop, calls=%fused_computation | loop fusion | flops 3145728 | bytes 8487424 | tf_op jit(solution)/shard_map/add | solution.py:50
  49.3 0.0 copy-start.1
  49.3 0.0 copy-start.15
  49.3 0.0 copy-start.10
  49.4 2.0 %copy-done.1 = f32[4,32,64,128]{3,2,1,0:T(8,128)} copy-done((f32[4,32,64,128]{3,2,1,0:T(8,128)}, f32[4,32,64,128]{3,2,1,0:T(8,128)S(1)}, u32[]{:S(2)}) %copy-start.1) | copy-done | bytes 4194328
  51.3 6.6 %fusion.13 = f32[4,32,1,64]{3,2,1,0:T(1,128)S(1)} fusion(f32[4,32,64,128]{3,2,1,0:T(8,128)S(1)} %multiply_add_fusion, f32[4,32,128,1]{2,3,1,0:T(1,128)S(1)} %bitcast.41), kind=kOutput, calls=%fused_computation.50 | convolution fusion | flops 12582912 | bytes 4292608 | tf_op jit(solution)/shard_map/shpn,shn->shp/dot_general | solution.py:53
  57.9 0.0 copy-done.15
  57.9 0.1 multiply_add_fusion.1
  58.0 0.1 reshape.81
  58.2 0.1 reduce_sum.84
  58.3 0.1 broadcast_bitcast_fusion
  58.4 0.0 copy-done.10
  58.4 14.0 %all-gather = bf16[8,4,2048]{2,1,0:T(4,128)(2,1)S(1)} all-gather(bf16[1,4,2048]{2,1,0:T(4,128)(2,1)S(1)} %fusion.10), channel_id=1, replica_groups=mesh['dp'=4,'kv'=4,'tp'=2] {'kv','tp'}, dimensions={0}, use_global_device_ids=true | all-gather | bytes 147456 | tf_op jit(solution)/shard_map/all_gather | solution.py:130
  72.4 2.0 %fusion.3 = f32[32,512]{1,0:T(8,128)S(1)} fusion(bf16[32,2048]{1,0:T(8,128)(2,1)S(1)} %reshape.83, bf16[2048,512]{1,0:T(8,128)(2,1)} %param.39, bf16[32,512]{1,0:T(8,128)(2,1)S(1)} %copy-done.2), kind=kOutput, calls=%fused_computation.8 | convolution fusion | flops 67190784 | bytes 2326528 | tf_op jit(solution)/shard_map/dot_general | solution.py:129
  74.5 14.9 %all_gather.7 = f32[32,4096]{1,0:T(8,128)S(1)} all-gather(f32[32,512]{1,0:T(8,128)S(1)} %fusion.3), channel_id=1, replica_groups=mesh['dp'=4,'kv'=4,'tp'=2] {'kv','tp'}, dimensions={1}, use_global_device_ids=true | all-gather | bytes 589824 | tf_op jit(solution)/shard_map/all_gather | solution.py:135
  89.4 0.2 reduce_sum.85
  89.6 0.2 multiply_reduce_fusion
  89.8 0.1 multiply_convert_fusion
  90.0 0.0 copy-start.9
  90.0 13.6 %fusion.4 = f32[32,4096]{1,0:T(8,128)S(1)} fusion(bf16[2048,4096]{1,0:T(8,128)(2,1)} %param.42, bf16[32,4096]{1,0:T(8,128)(2,1)S(1)} %multiply_convert_fusion, bf16[4096,2048]{1,0:T(8,128)(2,1)} %param.41), kind=kOutput, calls=%fused_computation.12 | convolution fusion | flops 1073938432 | bytes 34340864 | tf_op jit(solution)/shard_map/dot_general | solution.py:141
  103.6 32.5 %all-reduce.5 = bf16[32,4096]{1,0:T(8,128)(2,1)S(1)} all-reduce(f32[32,4096]{1,0:T(8,128)S(1)} %fusion.4), channel_id=3, replica_groups=mesh['dp'=4,'kv'=4,'tp'=2] {'kv','tp'}, use_global_device_ids=true, to_apply=%region_7.8.clone | all-reduce | flops 131072 | bytes 786432
  136.1 0.2 fusion.6
  136.3 0.2 multiply_reduce_fusion.2
  136.5 0.1 multiply_convert_fusion.1
  136.6 8.1 %all_to_all.19 = bf16[4,8,512]{2,0,1:T(4,128)(2,1)S(1)} all-to-all(bf16[4,8,512]{2,0,1:T(4,128)(2,1)S(1)} %bitcast.42), channel_id=1, replica_groups=mesh['dp'=4,'kv'=4,'tp'=2] {'kv','tp'}, dimensions={1} | all-to-all | bytes 65536 | tf_op jit(solution)/shard_map/all_to_all | solution.py:149
  144.8 0.6 all_to_all.17
  (28 shorter events, 0.4 us)
Async XLA Ops:
  0.6 1.8 %copy-start = (bf16[512,2048]{1,0:T(8,128)(2,1)S(1)}, bf16[512,2048]{1,0:T(8,128)(2,1)}, u32[]{:S(2)}) copy-start(bf16[512,2048]{1,0:T(8,128)(2,1)} %param.23) | copy-start | bytes 6291460
  0.7 43.1 %copy-start.18 = (u32[32]{0:T(128)S(1)}, u32[32]{0:T(128)}, u32[]{:S(2)}) copy-start(u32[32]{0:T(128)} %constant.53) | copy-start | bytes 388
  0.7 5.1 %copy-start.2 = (bf16[32,512]{1,0:T(8,128)(2,1)S(1)}, bf16[32,512]{1,0:T(8,128)(2,1)}, u32[]{:S(2)}) copy-start(bf16[32,512]{1,0:T(8,128)(2,1)} %param.22) | copy-start | bytes 98308
  0.7 5.1 %copy-start.3 = (bf16[512,256]{1,0:T(8,128)(2,1)S(1)}, bf16[512,256]{1,0:T(8,128)(2,1)}, u32[]{:S(2)}) copy-start(bf16[512,256]{1,0:T(8,128)(2,1)} %param.25) | copy-start | bytes 786436
  0.7 5.2 %copy-start.4 = (bf16[512,256]{1,0:T(8,128)(2,1)S(1)}, bf16[512,256]{1,0:T(8,128)(2,1)}, u32[]{:S(2)}) copy-start(bf16[512,256]{1,0:T(8,128)(2,1)} %param.26) | copy-start | bytes 786436
  0.7 5.4 %copy-start.6 = (bf16[512,32]{0,1:T(8,128)(2,1)S(1)}, bf16[512,32]{0,1:T(8,128)(2,1)}, u32[]{:S(2)}) copy-start(bf16[512,32]{0,1:T(8,128)(2,1)} %param.27) | copy-start | bytes 98308
  0.7 44.4 %copy-start.13 = (bf16[4,256]{1,0:T(4,128)(2,1)S(1)}, bf16[4,256]{1,0:T(4,128)(2,1)}, u32[]{:S(2)}) copy-start(bf16[4,256]{1,0:T(4,128)(2,1)} %param.29) | copy-start | bytes 6148
  0.7 44.4 %copy-start.14 = (bf16[4,256]{1,0:T(4,128)(2,1)S(1)}, bf16[4,256]{1,0:T(4,128)(2,1)}, u32[]{:S(2)}) copy-start(bf16[4,256]{1,0:T(4,128)(2,1)} %param.30) | copy-start | bytes 6148
  0.7 44.4 %copy-start.12 = (bf16[4,3,256]{2,0,1:T(4,128)(2,1)S(1)}, bf16[4,3,256]{2,0,1:T(4,128)(2,1)}, u32[]{:S(2)}) copy-start(bf16[4,3,256]{2,0,1:T(4,128)(2,1)} %param.32) | copy-start | bytes 18436
  0.7 44.4 %copy-start.11 = (bf16[4,3,256]{2,0,1:T(4,128)(2,1)S(1)}, bf16[4,3,256]{2,0,1:T(4,128)(2,1)}, u32[]{:S(2)}) copy-start(bf16[4,3,256]{2,0,1:T(4,128)(2,1)} %param.33) | copy-start | bytes 18436
  0.7 44.4 %copy-start.7 = (bf16[4,2048]{1,0:T(4,128)(2,1)S(1)}, bf16[4,2048]{1,0:T(4,128)(2,1)}, u32[]{:S(2)}) copy-start(bf16[4,2048]{1,0:T(4,128)(2,1)} %param.28) | copy-start | bytes 49156
  0.8 44.5 %copy-start.5 = (bf16[4,3,2048]{2,0,1:T(4,128)(2,1)S(1)}, bf16[4,3,2048]{2,0,1:T(4,128)(2,1)}, u32[]{:S(2)}) copy-start(bf16[4,3,2048]{2,0,1:T(4,128)(2,1)} %param.31) | copy-start | bytes 147460
  0.8 44.6 %copy-start.17 = (f32[32]{0:T(128)S(1)}, f32[32]{0:T(128)}, u32[]{:S(2)}) copy-start(f32[32]{0:T(128)} %param.35) | copy-start | bytes 388
  0.8 44.7 %copy-start.16 = (f32[32]{0:T(128)S(1)}, f32[32]{0:T(128)}, u32[]{:S(2)}) copy-start(f32[32]{0:T(128)} %param.34) | copy-start | bytes 388
  49.3 2.0 %copy-start.1 = (f32[4,32,64,128]{3,2,1,0:T(8,128)}, f32[4,32,64,128]{3,2,1,0:T(8,128)S(1)}, u32[]{:S(2)}) copy-start(f32[4,32,64,128]{3,2,1,0:T(8,128)S(1)} %multiply_add_fusion) | copy-start | bytes 12582916
  49.3 8.6 %copy-start.15 = (f32[32]{0:T(128)S(1)}, f32[32]{0:T(128)}, u32[]{:S(2)}) copy-start(f32[32]{0:T(128)} %param.36) | copy-start | bytes 388
  49.3 9.1 %copy-start.10 = (f32[2048]{0:T(1024)S(1)}, f32[2048]{0:T(1024)}, u32[]{:S(2)}) copy-start(f32[2048]{0:T(1024)} %param.38) | copy-start | bytes 24580
  51.3 38.5 %copy-start.8 = (f32[4096]{0:T(1024)S(1)}, f32[4096]{0:T(1024)}, u32[]{:S(2)}) copy-start(f32[4096]{0:T(1024)} %param.40) | copy-start | bytes 49156
  90.0 46.6 %copy-start.9 = (f32[4096]{0:T(1024)S(1)}, f32[4096]{0:T(1024)}, u32[]{:S(2)}) copy-start(f32[4096]{0:T(1024)} %param.43) | copy-start | bytes 49156
where the time goes:
time: 146 us; the launch traced here: 145 us
  blocking collectives  107 us (73%)
  matrix products  25.9 us (18%)
  local copies, waits for them, and re-layouts  5.37 us (4%)
  other arithmetic  5.27 us (4%)
  between operations  1.74 us (1%)
    unnamed x2, blocking collectives  70.1 us
    all_gather x1, blocking collectives, on_device(): whole_residual = lax.all_gather(residual, ('kv', 'tp'), axis=1, tiled=True)  14.9 us
    all_gather x1, blocking collectives, on_device(): lax.all_gather(mixed, ('kv', 'tp'), axis=0, tiled=True)  14 us
    dot_general x1, matrix products, on_device(): jnp.dot(hidden, down_weight, preferred_element_type=jnp.float32)  13.6 us
    all_to_all x1, blocking collectives, on_device(): lax.all_to_all(finished, ('kv', 'tp'), split_axis=1, concat_axis=0, tiled...  8.12 us
    dot_general x1, matrix products, mixer_step(): jnp.einsum('shpn,shn->shp', state_next, reads_head, precision=lax.Precisi...  6.59 us
    unnamed x42, local copies, waits for them, and re-layouts  4.42 us
    add x1, other arithmetic, mixer_step(): decays[:, :, None, None] * state_past  3.73 us

commit v1 on v0

v1 whole, which is shorter than its diff:
```python
import functools

import jax
import jax.numpy as jnp
from jax import lax
from jax.experimental import pallas as pl
from jax.experimental.pallas import tpu as pltpu
from jax.sharding import PartitionSpec as P

HEADS = 32
HEAD_DIM = 64
STATE_DIM = 128
GROUPS = 2

RESIDUAL_SCALE = 2.0**0.25
NORM_EPSILON = 1e-05
MIXER_EPSILON = 1e-06

F32 = jnp.float32
BF16 = jnp.bfloat16
ANY = pl.BlockSpec(memory_space=pl.ANY)
VMEM = pl.BlockSpec(memory_space=pltpu.VMEM)


def silu(v):
    return v * jax.nn.sigmoid(v)


def layer_kernel(geo, *refs):
    n, tp_size, seqs, rows, width, offsets, ways, halves = geo
    inputs = refs[:22]
    layer_out, decay_out, drive_out, write_out = refs[22:26]
    held = refs[26:48]
    (
        wide, send1, recv1, spread, read_out, mix_all, mix_rows, res_all, normed_f, own_normed,
        normed_b, hidden, down_rows, send2, recv2, finished, done_all, done_rows,
        load_sem, s1, r1, s2, r2, s3, r3, s4, r4, s5, r5,
    ) = refs[48:]
    (
        x, gate_w, value_w, write_w, read_w, step_w, value_taps, write_taps, read_taps, past_values,
        past_writes, past_reads, step_bias, decay_log, skip_scale, state, mixer_gain, out_w, gain1,
        up_w, down_w, gain2,
    ) = held
    inner = value_w.shape[1]
    model = gain1.shape[1]
    cols = x.shape[1]
    me = lax.axis_index("kv") * tp_size + lax.axis_index("tp")

    def peer(step):
        other = lax.rem(me + step, n)
        return other, {"kv": lax.div(other, tp_size), "tp": lax.rem(other, tp_size)}

    loads = {}
    count = 0
    for i in range(22):
        parts = ways if i in (19, 20) else 1
        depth = inputs[i].shape[0] // parts
        loads[i] = []
        for part in range(parts):
            if parts == 1:
                src, dst = inputs[i], held[i]
            else:
                src = inputs[i].at[pl.ds(part * depth, depth)]
                dst = held[i].at[pl.ds(part * depth, depth)]
            loads[i].append(pltpu.make_async_copy(src, dst, load_sem.at[count]))
            count += 1

    def start(*which):
        for i in which:
            for copy in loads[i]:
                copy.start()

    def wait(*which):
        for i in which:
            for copy in loads[i]:
                copy.wait()

    start(0, 5, 3, 4, 2, 1)
    start(6, 7, 8, 9, 10, 11, 12, 13, 14, 16, 18, 21)
    start(15)

    barrier = pltpu.get_barrier_semaphore()
    for j in range(1, n):
        pl.semaphore_signal(
            barrier, inc=1, device_id=peer(j)[1], device_id_type=pl.DeviceIdType.MESH
        )

    def exchange(source, target, send_sem, recv_sem):
        copies = []
        for j in range(1, n):
            other, where = peer(j)
            copy = pltpu.make_async_remote_copy(
                src_ref=source(other),
                dst_ref=target(j),
                send_sem=send_sem.at[j],
                recv_sem=recv_sem.at[j],
                device_id=where,
                device_id_type=pl.DeviceIdType.MESH,
            )
            copy.start()
            copies.append(copy)
        return copies

    wait(0)
    wide[:, offsets[4] :] = jnp.zeros((rows, width - offsets[4]), F32)
    order = (5, 3, 4, 2, 1)
    for place, i in enumerate(order):
        wait(i)
        if place == len(order) - 1:
            start(17, 19, 20)
        w = held[i]
        for begin in range(0, w.shape[1], 512):
            size = min(512, w.shape[1] - begin)
            wide[:, offsets[i - 1] + begin : offsets[i - 1] + begin + size] = jnp.dot(
                x[...], w[:, begin : begin + size], preferred_element_type=F32
            )
    for d in range(n):
        send1[d] = wide[d * seqs : (d + 1) * seqs, :].astype(BF16)
    pl.semaphore_wait(barrier, n - 1)
    first = exchange(lambda other: send1.at[other], lambda j: recv1.at[j], s1, r1)

    wait(6, 7, 8, 9, 10, 11, 12, 13, 14, 16, 18, 21, 15)
    head_of = lax.broadcasted_iota(jnp.int32, (HEADS, inner), 1) // HEAD_DIM
    spreader = (head_of == lax.broadcasted_iota(jnp.int32, (HEADS, inner), 0)).astype(F32)

    total = send1[me].astype(F32)
    for j in range(1, n):
        first[j - 1].wait_recv()
        total = total + recv1[j].astype(F32)
    total = total.astype(BF16).astype(F32)

    def conv(now, past, taps):
        t = taps[...].astype(F32)
        p = past[...].astype(F32)
        acc = now * t[3:4]
        for k in range(3):
            acc = acc + p[:, k, :] * t[k : k + 1]
        return silu(acc)

    groups = GROUPS * STATE_DIM
    gate = total[:, offsets[0] : offsets[0] + inner]
    values = conv(total[:, offsets[1] : offsets[1] + inner], past_values, value_taps)
    writes = conv(total[:, offsets[2] : offsets[2] + groups], past_writes, write_taps)
    reads = conv(total[:, offsets[3] : offsets[3] + groups], past_reads, read_taps)
    raw = total[:, offsets[4] : offsets[4] + HEADS] + step_bias[...]
    step_size = jnp.maximum(raw, 0.0) + jnp.log1p(jnp.exp(-jnp.abs(raw)))
    decays = jnp.exp(-step_size * jnp.exp(decay_log[...]))
    pad = spread.shape[0] // 3
    spread[...] = jnp.zeros(spread.shape, F32)
    spread[0:seqs, :] = step_size
    spread[pad : pad + seqs, :] = decays
    spread[2 * pad : 2 * pad + 1, :] = skip_scale[...]
    per_channel = jnp.dot(
        spread[...], spreader, preferred_element_type=F32, precision=lax.Precision.HIGHEST
    )
    step_c = per_channel[0:seqs]
    decay_c = per_channel[pad : pad + seqs]
    skip_c = per_channel[2 * pad : 2 * pad + 1]
    half = inner // GROUPS
    for g in range(GROUPS):
        reads_g = reads[:, g * STATE_DIM : (g + 1) * STATE_DIM].astype(BF16)
        for s in range(seqs):
            block = state[s, g * half : (g + 1) * half, :].astype(BF16)
            seen = lax.dot_general(
                reads_g, block, (((1,), (1,)), ((), ())), preferred_element_type=F32
            )
            read_out[s : s + 1, g * half : (g + 1) * half] = seen[s : s + 1]
    drive = step_c * values
    decay_out[...] = jnp.zeros(decay_out.shape, F32)
    drive_out[...] = jnp.zeros(drive_out.shape, F32)
    write_out[...] = jnp.zeros(write_out.shape, F32)
    decay_out[0:seqs, :] = decay_c
    drive_out[0:seqs, :] = drive
    write_out[0:seqs, :] = writes
    base = decay_c * read_out[...] + skip_c * values
    gate_act = silu(gate)
    product = writes * reads
    for g in range(GROUPS):
        here = slice(g * half, (g + 1) * half)
        overlap = jnp.sum(product[:, g * STATE_DIM : (g + 1) * STATE_DIM], -1, keepdims=True)
        gated = (base[:, here] + drive[:, here] * overlap) * gate_act[:, here]
        scale = lax.rsqrt(jnp.mean(gated * gated, -1, keepdims=True) + MIXER_EPSILON)
        mix_all[me, :, here] = (gated * scale * mixer_gain[:, here]).astype(BF16)
    second = exchange(lambda other: mix_all.at[me], lambda j: mix_all.at[me], s2, r2)

    wait(17)
    for copy in second:
        copy.wait_recv()
    for d in range(n):
        mix_rows[d * seqs : (d + 1) * seqs, :] = mix_all[d].astype(F32)
    mix_out = jnp.dot(mix_rows[...].astype(BF16), out_w[...], preferred_element_type=F32)
    residual = RESIDUAL_SCALE * x[...].astype(F32) + mix_out.astype(BF16).astype(F32)
    res_all[me] = residual.astype(BF16)
    third = exchange(lambda other: res_all.at[me], lambda j: res_all.at[me], s3, r3)

    wait(19, 20)
    for copy in third:
        copy.wait_recv()
    total1 = jnp.zeros((rows, 1), F32)
    for d in range(n):
        total1 = total1 + jnp.sum(res_all[d].astype(F32), -1, keepdims=True)
    average = total1 / model
    total2 = jnp.zeros((rows, 1), F32)
    for d in range(n):
        off = res_all[d].astype(F32) - average
        total2 = total2 + jnp.sum(off * off, -1, keepdims=True)
    scale = lax.rsqrt(total2 / model + NORM_EPSILON)
    for d in range(n):
        here = slice(d * cols, (d + 1) * cols)
        block = (res_all[d].astype(F32) - average) * scale * gain1[:, here]
        normed_b[:, here] = block.astype(BF16)
        normed_f[:, here] = block.astype(BF16).astype(F32)
    for d in range(n):

        @pl.when(me == d)
        def _():
            own_normed[...] = normed_f[d * seqs : (d + 1) * seqs, :]

    chunk = min(256, up_w.shape[1])

    @pl.loop(0, up_w.shape[1] // chunk)
    def _(c):
        here = pl.ds(pl.multiple_of(c * chunk, chunk), chunk)
        h = jnp.dot(normed_b[...], up_w[:, here], preferred_element_type=F32)
        h = jnp.maximum(h, 0.0)
        hidden[:, here] = (h * h).astype(BF16)

    span = model // halves
    fourth = []
    for part in range(halves):

        @pl.loop(0, span // 512)
        def _(c):
            there = pl.ds(pl.multiple_of(c * 512, 512), 512)
            here = pl.ds(pl.multiple_of(part * span + c * 512, 512), 512)
            down_rows[:, there] = jnp.dot(
                hidden[...], down_w[:, here], preferred_element_type=F32
            )

        for d in range(n):
            send2[part, d] = down_rows[d * seqs : (d + 1) * seqs, :].astype(BF16)
        fourth.append(
            exchange(
                lambda other: send2.at[part, other],
                lambda j: recv2.at[part, j],
                s4.at[part],
                r4.at[part],
            )
        )

    rows2 = []
    for part in range(halves):
        channel = send2[part, me].astype(F32)
        for j in range(1, n):
            fourth[part][j - 1].wait_recv()
            channel = channel + recv2[part, j].astype(F32)
        rows2.append(
            RESIDUAL_SCALE * own_normed[:, part * span : (part + 1) * span]
            + channel.astype(BF16).astype(F32)
        )
    average = sum(jnp.sum(r, -1, keepdims=True) for r in rows2) / model
    rows2 = [r - average for r in rows2]
    variance = sum(jnp.sum(r * r, -1, keepdims=True) for r in rows2) / model
    scale = lax.rsqrt(variance + NORM_EPSILON)
    for d in range(n):
        part, begin = divmod(d * cols, span)
        block = rows2[part][:, begin : begin + cols] * scale * gain2[:, d * cols : (d + 1) * cols]
        finished[d] = block.astype(BF16)
    done_all[me] = finished[me]
    fifth = exchange(lambda other: finished.at[other], lambda j: done_all.at[me], s5, r5)
    for copy in fifth:
        copy.wait_recv()
    for d in range(n):
        done_rows[d * seqs : (d + 1) * seqs, :] = done_all[d].astype(F32)
    layer_out[...] = done_rows[...].astype(BF16)
    for group in [first, second, third, *fourth, fifth]:
        for copy in group:
            copy.wait_send()


def state_kernel(seqs, state, decay, drive, write, layer_in, state_out, layer_out):
    decay_t = jnp.transpose(decay[...])
    drive_t = jnp.transpose(drive[...])
    for s in range(seqs):
        state_out[s] = decay_t[:, s : s + 1] * state[s] + drive_t[:, s : s + 1] * write[s : s + 1, :]
    layer_out[...] = layer_in[...]


def on_device(n, tp_size, *args):
    x = args[0]
    state = args[15]
    seqs, rows, cols = state.shape[0], x.shape[0], x.shape[1]
    inner = args[1].shape[1]
    model = args[18].shape[0]
    hidden_here = args[19].shape[1]
    offsets = [0]
    for i in range(1, 5):
        offsets.append(offsets[-1] + args[i].shape[1])
    width = offsets[-1] + 128
    args = list(args)
    args[15] = state.reshape(seqs, inner, STATE_DIM)
    for i in (12, 13, 14, 16, 18, 21):
        args[i] = args[i].reshape(1, -1)
    ways, halves = 4, 2
    pad = (seqs + 7) // 8 * 8
    dma = pltpu.SemaphoreType.DMA
    scratch = [pltpu.VMEM(a.shape, a.dtype) for a in args]
    scratch += [
        pltpu.VMEM((rows, width), F32),
        pltpu.VMEM((n, seqs, width), BF16),
        pltpu.VMEM((n, seqs, width), BF16),
        pltpu.VMEM((3 * pad, HEADS), F32),
        pltpu.VMEM((seqs, inner), F32),
        pltpu.VMEM((n, seqs, inner), BF16),
        pltpu.VMEM((rows, inner), F32),
        pltpu.VMEM((n, rows, cols), BF16),
        pltpu.VMEM((rows, model), F32),
        pltpu.VMEM((seqs, model), F32),
        pltpu.VMEM((rows, model), BF16),
        pltpu.VMEM((rows, hidden_here), BF16),
        pltpu.VMEM((rows, model // halves), F32),
        pltpu.VMEM((halves, n, seqs, model // halves), BF16),
        pltpu.VMEM((halves, n, seqs, model // halves), BF16),
        pltpu.VMEM((n, seqs, cols), BF16),
        pltpu.VMEM((n, seqs, cols), BF16),
        pltpu.VMEM((rows, cols), F32),
        dma((20 + 2 * ways,)),
        dma((n,)), dma((n,)), dma((n,)), dma((n,)), dma((n,)), dma((n,)),
        dma((halves, n)), dma((halves, n)), dma((n,)), dma((n,)),
    ]
    geo = (n, tp_size, seqs, rows, width, tuple(offsets), ways, halves)
    layer_rows, decay, drive, write = pl.pallas_call(
        functools.partial(layer_kernel, geo),
        out_shape=(
            jax.ShapeDtypeStruct((rows, cols), BF16),
            jax.ShapeDtypeStruct((pad, inner), F32),
            jax.ShapeDtypeStruct((pad, inner), F32),
            jax.ShapeDtypeStruct((pad, GROUPS * STATE_DIM), F32),
        ),
        in_specs=[ANY] * 22,
        out_specs=(VMEM,) * 4,
        scratch_shapes=scratch,
        compiler_params=pltpu.CompilerParams(
            collective_id=0, has_side_effects=True, vmem_limit_bytes=60 * 1024 * 1024
        ),
        name="layer",
    )(*args)
    block = 256
    per_group = inner // GROUPS // block
    state_next, result = pl.pallas_call(
        functools.partial(state_kernel, seqs),
        grid=(inner // block,),
        in_specs=[
            pl.BlockSpec((seqs, block, STATE_DIM), lambda i: (0, i, 0)),
            pl.BlockSpec((pad, block), lambda i: (0, i)),
            pl.BlockSpec((pad, block), lambda i: (0, i)),
            pl.BlockSpec((pad, STATE_DIM), lambda i: (0, i // per_group)),
            pl.BlockSpec((rows, cols), lambda i: (0, 0)),
        ],
        out_specs=(
            pl.BlockSpec((seqs, block, STATE_DIM), lambda i: (0, i, 0)),
            pl.BlockSpec((rows, cols), lambda i: (0, 0)),
        ),
        out_shape=(
            jax.ShapeDtypeStruct((seqs, inner, STATE_DIM), F32),
            jax.ShapeDtypeStruct((rows, cols), BF16),
        ),
        name="state",
    )(args[15], decay, drive, write, layer_rows)
    return result, state_next.reshape(state.shape)


def solution(mesh):
    tp_size = mesh.shape["tp"]
    n = mesh.shape["kv"] * tp_size
    split, whole = P(("kv", "tp"), None), P()
    past = P(("dp", "kv", "tp"), None, None)
    states = P(("dp", "kv", "tp"), None, None, None)
    columns = P(None, ("kv", "tp"))
    placed = (
        (P("dp", ("kv", "tp")),) + (split,) * 5 + (whole,) * 3 + (past,) * 3 + (whole,) * 3
        + (states, whole, columns, whole, columns, split, whole)
    )
    return jax.shard_map(
        functools.partial(on_device, n, tp_size),
        mesh=mesh,
        in_specs=placed,
        out_specs=(P("dp", ("kv", "tp")), states),
        check_vma=False,
    )
```

time: 146 us -> 60.3 us (0.41)
  blocking collectives: 107 us -> 0 us
  Pallas kernels: 0 us -> 53.7 us
  matrix products: 25.9 us -> 0 us
  other arithmetic: 5.27 us -> 0 us
    unnamed x2 -> x0, blocking collectives: 70.1 us -> none
    pallas_call x0 -> x2, Pallas kernels: none -> 53.7 us  [the longest x1 45.5 us: on_device(): pl.pallas_call(functools.partial(layer_kernel, geo), out_shape=(jax.Shape...]
    all_gather x2 -> x0, blocking collectives: 28.9 us -> none  [the longest x1 14.9 us: on_device(): whole_residual = lax.all_gather(residual, ('kv', 'tp'), axis=1, tiled=True)]
    dot_general x8 -> x0, matrix products: 25.9 us -> none  [the longest x1 13.6 us: on_device(): jnp.dot(hidden, down_weight, preferred_element_type=jnp.float32)]
    all_to_all x1 -> x0, blocking collectives: 8.12 us -> none  [on_device(): lax.all_to_all(finished, ('kv', 'tp'), split_axis=1, concat_axis=0, tiled...]
    add x2 -> x0, other arithmetic: 3.81 us -> none  [the longest x1 3.73 us: mixer_step(): decays[:, :, None, None] * state_past]
    unnamed x42 -> x4, local copies, waits for them, and re-layouts: 4.42 us -> 5.55 us
where the time goes in v1:
time: 60.3 us; the launch traced here: 59.9 us
  Pallas kernels  53.7 us (89%)
  local copies, waits for them, and re-layouts  5.55 us (9%)
  between operations  0.64 us (1%)
    pallas_call x1, Pallas kernels, on_device(): pl.pallas_call(functools.partial(layer_kernel, geo), out_shape=(jax.Shape...  45.5 us
    pallas_call x1, Pallas kernels, on_device(): pl.pallas_call(functools.partial(state_kernel, seqs), grid=(inner // bloc...  8.18 us
    unnamed x4, local copies, waits for them, and re-layouts  5.55 us

profile of v1, /device:TPU:0, one launch (start us, length us, event | category | flops | bytes accessed | tf_op | source)
XLA Modules:
  0.0 59.9 jit_solution(16597201480861525087)
XLA Ops:
  0.6 1.3 %copy.26.refs_10_ = bf16[4,3,256]{2,1,0:T(4,128)(2,1)} copy(bf16[4,3,256]{2,0,1:T(4,128)(2,1)} %param.32) | data formatting | bytes 12288 | tf_op args[10]
  1.9 1.3 %copy.27.refs_11_ = bf16[4,3,256]{2,1,0:T(4,128)(2,1)} copy(bf16[4,3,256]{2,0,1:T(4,128)(2,1)} %param.33) | data formatting | bytes 12288 | tf_op args[11]
  3.2 1.5 %copy.25.refs_9_ = bf16[4,3,2048]{2,1,0:T(4,128)(2,1)} copy(bf16[4,3,2048]{2,0,1:T(4,128)(2,1)} %param.31) | data formatting | bytes 98304 | tf_op args[9]
  4.7 1.5 %copy.24.refs_5_ = bf16[512,32]{1,0:T(8,128)(2,1)} copy(bf16[512,32]{0,1:T(8,128)(2,1)} %param.27) | data formatting | bytes 65536 | tf_op args[5]
  6.2 45.5 %layer.1 = (bf16[32,512]{1,0:T(8,128)(2,1)}, f32[8,2048]{1,0:T(8,128)}, f32[8,2048]{1,0:T(8,128)}, f32[8,256]{1,0:T(8,128)}) custom-call(bf16[32,512]{1,0:T(8,128)(2,1)} %refs_0_.1, bf16[512,2048]{1,0:T(8,128)(2,1)} %refs_1_.1, bf16[512,2048]{1,0:T(8,128)(2,1)} %refs_2_.1, bf16[512,256]{1,0:T(8,128)(2,1)} %refs_3_.1, bf16[512,256]{1,0:T(8,128)(2,1)} %refs_4_.1, ...), custom_call_target="tpu_custom_call" | custom-call | tf_op jit(solution)/shard_map/layer/pallas_call | solution.py:332
  51.7 8.2 %state.1 = (f32[4,2048,128]{2,1,0:T(8,128)}, bf16[32,512]{1,0:T(8,128)(2,1)}) custom-call(f32[4,2048,128]{2,1,0:T(8,128)} %bitcast.9, f32[8,2048]{1,0:T(8,128)} %get-tuple-element.8.decay, f32[8,2048]{1,0:T(8,128)} %get-tuple-element.9.drive, f32[8,256]{1,0:T(8,128)} %get-tuple-element.10.write, bf16[32,512]{1,0:T(8,128)(2,1)} %get-tuple-element.11.layer_in), custom_call_target="tpu_custom_call" | custom-call | tf_op jit(solution)/shard_map/state/pallas_call | solution.py:350

commit v2 on v1

--- a/solution.py
+++ b/solution.py
@@ -29,13 +29,14 @@
 def layer_kernel(geo, *refs):
     n, tp_size, seqs, rows, width, offsets, ways, halves = geo
     inputs = refs[:22]
-    layer_out, decay_out, drive_out, write_out = refs[22:26]
-    held = refs[26:48]
+    layer_out, state_out = refs[22:24]
+    held = refs[24:46]
+    decay_out, drive_out, write_out = refs[46:49]
     (
         wide, send1, recv1, spread, read_out, mix_all, mix_rows, res_all, normed_f, own_normed,
         normed_b, hidden, down_rows, send2, recv2, finished, done_all, done_rows,
-        load_sem, s1, r1, s2, r2, s3, r3, s4, r4, s5, r5,
-    ) = refs[48:]
+        load_sem, store_sem, s1, r1, s2, r2, s3, r3, s4, r4, s5, r5,
+    ) = refs[49:]
     (
         x, gate_w, value_w, write_w, read_w, step_w, value_taps, write_taps, read_taps, past_values,
         past_writes, past_reads, step_bias, decay_log, skip_scale, state, mixer_gain, out_w, gain1,
@@ -109,6 +110,11 @@
         if place == len(order) - 1:
             start(17, 19, 20)
         w = held[i]
+        if i == 5:
+            wide[:, offsets[4] : offsets[4] + HEADS] = lax.dot_general(
+                x[...], w[...], (((1,), (1,)), ((), ())), preferred_element_type=F32
+            )
+            continue
         for begin in range(0, w.shape[1], 512):
             size = min(512, w.shape[1] - begin)
             wide[:, offsets[i - 1] + begin : offsets[i - 1] + begin + size] = jnp.dot(
@@ -134,7 +140,7 @@
         p = past[...].astype(F32)
         acc = now * t[3:4]
         for k in range(3):
-            acc = acc + p[:, k, :] * t[k : k + 1]
+            acc = acc + p[k] * t[k : k + 1]
         return silu(acc)
 
     groups = GROUPS * STATE_DIM
@@ -183,6 +189,30 @@
         mix_all[me, :, here] = (gated * scale * mixer_gain[:, here]).astype(BF16)
     second = exchange(lambda other: mix_all.at[me], lambda j: mix_all.at[me], s2, r2)
 
+    strip = 256
+    stores = []
+
+    def update_states(g):
+        @pl.loop(0, half // strip)
+        def _(b):
+            here = pl.ds(pl.multiple_of(g * half + b * strip, strip), strip)
+            decay_t = jnp.transpose(decay_out[:, here])
+            drive_t = jnp.transpose(drive_out[:, here])
+            for s in range(seqs):
+                write = write_out[s : s + 1, g * STATE_DIM : (g + 1) * STATE_DIM]
+                state[s, here, :] = (
+                    decay_t[:, s : s + 1] * state[s, here, :] + drive_t[:, s : s + 1] * write
+                )
+
+        where = pl.ds(g * half, half)
+        store = pltpu.make_async_copy(
+            state.at[:, where], state_out.at[:, where], store_sem.at[g]
+        )
+        store.start()
+        stores.append(store)
+
+    update_states(0)
+
     wait(17)
     for copy in second:
         copy.wait_recv()
@@ -192,6 +222,8 @@
     residual = RESIDUAL_SCALE * x[...].astype(F32) + mix_out.astype(BF16).astype(F32)
     res_all[me] = residual.astype(BF16)
     third = exchange(lambda other: res_all.at[me], lambda j: res_all.at[me], s3, r3)
+    for g in range(1, GROUPS):
+        update_states(g)
 
     wait(19, 20)
     for copy in third:
@@ -273,17 +305,11 @@
     for d in range(n):
         done_rows[d * seqs : (d + 1) * seqs, :] = done_all[d].astype(F32)
     layer_out[...] = done_rows[...].astype(BF16)
+    for store in stores:
+        store.wait()
     for group in [first, second, third, *fourth, fifth]:
         for copy in group:
             copy.wait_send()
-
-
-def state_kernel(seqs, state, decay, drive, write, layer_in, state_out, layer_out):
-    decay_t = jnp.transpose(decay[...])
-    drive_t = jnp.transpose(drive[...])
-    for s in range(seqs):
-        state_out[s] = decay_t[:, s : s + 1] * state[s] + drive_t[:, s : s + 1] * write[s : s + 1, :]
-    layer_out[...] = layer_in[...]
 
 
 def on_device(n, tp_size, *args):
@@ -299,6 +325,9 @@
     width = offsets[-1] + 128
     args = list(args)
     args[15] = state.reshape(seqs, inner, STATE_DIM)
+    args[5] = args[5].T
+    for i in (9, 10, 11):
+        args[i] = jnp.transpose(args[i], (1, 0, 2))
     for i in (12, 13, 14, 16, 18, 21):
         args[i] = args[i].reshape(1, -1)
     ways, halves = 4, 2
@@ -306,6 +335,9 @@
     dma = pltpu.SemaphoreType.DMA
     scratch = [pltpu.VMEM(a.shape, a.dtype) for a in args]
     scratch += [
+        pltpu.VMEM((pad, inner), F32),
+        pltpu.VMEM((pad, inner), F32),
+        pltpu.VMEM((pad, GROUPS * STATE_DIM), F32),
         pltpu.VMEM((rows, width), F32),
         pltpu.VMEM((n, seqs, width), BF16),
         pltpu.VMEM((n, seqs, width), BF16),
@@ -325,48 +357,25 @@
         pltpu.VMEM((n, seqs, cols), BF16),
         pltpu.VMEM((rows, cols), F32),
         dma((20 + 2 * ways,)),
+        dma((GROUPS,)),
         dma((n,)), dma((n,)), dma((n,)), dma((n,)), dma((n,)), dma((n,)),
         dma((halves, n)), dma((halves, n)), dma((n,)), dma((n,)),
     ]
     geo = (n, tp_size, seqs, rows, width, tuple(offsets), ways, halves)
-    layer_rows, decay, drive, write = pl.pallas_call(
+    result, state_next = pl.pallas_call(
         functools.partial(layer_kernel, geo),
         out_shape=(
             jax.ShapeDtypeStruct((rows, cols), BF16),
-            jax.ShapeDtypeStruct((pad, inner), F32),
-            jax.ShapeDtypeStruct((pad, inner), F32),
-            jax.ShapeDtypeStruct((pad, GROUPS * STATE_DIM), F32),
+            jax.ShapeDtypeStruct((seqs, inner, STATE_DIM), F32),
         ),
         in_specs=[ANY] * 22,
-        out_specs=(VMEM,) * 4,
+        out_specs=(VMEM, ANY),
         scratch_shapes=scratch,
         compiler_params=pltpu.CompilerParams(
-            collective_id=0, has_side_effects=True, vmem_limit_bytes=60 * 1024 * 1024
+            collective_id=0, has_side_effects=True, vmem_limit_bytes=67043328
         ),
         name="layer",
     )(*args)
-    block = 256
-    per_group = inner // GROUPS // block
-    state_next, result = pl.pallas_call(
-        functools.partial(state_kernel, seqs),
-        grid=(inner // block,),
-        in_specs=[
-            pl.BlockSpec((seqs, block, STATE_DIM), lambda i: (0, i, 0)),
-            pl.BlockSpec((pad, block), lambda i: (0, i)),
-            pl.BlockSpec((pad, block), lambda i: (0, i)),
-            pl.BlockSpec((pad, STATE_DIM), lambda i: (0, i // per_group)),
-            pl.BlockSpec((rows, cols), lambda i: (0, 0)),
-        ],
-        out_specs=(
-            pl.BlockSpec((seqs, block, STATE_DIM), lambda i: (0, i, 0)),
-            pl.BlockSpec((rows, cols), lambda i: (0, 0)),
-        ),
-        out_shape=(
-            jax.ShapeDtypeStruct((seqs, inner, STATE_DIM), F32),
-            jax.ShapeDtypeStruct((rows, cols), BF16),
-        ),
-        name="state",
-    )(args[15], decay, drive, write, layer_rows)
     return result, state_next.reshape(state.shape)
 
 

time: 60.3 us -> 52.5 us (0.87)
  Pallas kernels: 53.7 us -> 45.5 us
  local copies, waits for them, and re-layouts: 5.55 us -> 6.16 us
    pallas_call x1 -> x0, Pallas kernels: 8.18 us -> none  [on_device(): pl.pallas_call(functools.partial(state_kernel, seqs), grid=(inner // bloc...]
    unnamed x4 -> x2, local copies, waits for them, and re-layouts: 5.55 us -> 6.16 us
where the time goes in v2:
time: 52.5 us; the launch traced here: 52.3 us
  Pallas kernels  45.5 us (87%)
  local copies, waits for them, and re-layouts  6.16 us (12%)
  between operations  0.65 us (1%)
    pallas_call x1, Pallas kernels, on_device(): pl.pallas_call(functools.partial(layer_kernel, geo), out_shape=(jax.Shape...  45.5 us
    unnamed x2, local copies, waits for them, and re-layouts  6.16 us

profile of v2, /device:TPU:0, one launch (start us, length us, event | category | flops | bytes accessed | tf_op | source)
XLA Modules:
  0.0 52.3 jit_solution(18309473870483992023)
XLA Ops:
  0.6 45.5 %layer.1 = (bf16[32,512]{1,0:T(8,128)(2,1)}, f32[4,2048,128]{2,1,0:T(8,128)}) custom-call(bf16[32,512]{1,0:T(8,128)(2,1)} %refs_0_.1, bf16[512,2048]{1,0:T(8,128)(2,1)} %refs_1_.1, bf16[512,2048]{1,0:T(8,128)(2,1)} %refs_2_.1, bf16[512,256]{1,0:T(8,128)(2,1)} %refs_3_.1, bf16[512,256]{1,0:T(8,128)(2,1)} %refs_4_.1, bf16[32,512]{1,0:T(8,128)(2,1)} %bitcast.15, ...), custom_call_target="tpu_custom_call" | custom-call | tf_op jit(solution)/shard_map/layer/pallas_call | solution.py:365
  46.1 1.4 %copy.26 = bf16[32,512]{1,0:T(8,128)(2,1)} copy(bf16[32,512]{1,0:T(8,128)(2,1)} %get-tuple-element.8) | data formatting | bytes 65536
  47.5 4.8 %copy.27 = f32[4,32,64,128]{3,2,1,0:T(8,128)} copy(f32[4,32,64,128]{3,2,1,0:T(8,128)} %bitcast.13) | data formatting | bytes 8388608

commit v3 on v2

--- a/solution.py
+++ b/solution.py
@@ -33,9 +33,10 @@
     held = refs[24:46]
     decay_out, drive_out, write_out = refs[46:49]
     (
-        wide, send1, recv1, spread, read_out, mix_all, mix_rows, res_all, normed_f, own_normed,
+        wide, send1, recv1, send_gate, recv_gate, spread, read_out, mix_all, mix_rows, res_all, normed_f, own_normed,
         normed_b, hidden, down_rows, send2, recv2, finished, done_all, done_rows,
-        load_sem, store_sem, s1, r1, s2, r2, s3, r3, s4, r4, s5, r5,
+        load_sem, store_sem, s1, r1, s2, r2, s3, r3, s4, r4, s5, r5, s6, r6,
+        s7, r7,
     ) = refs[49:]
     (
         x, gate_w, value_w, write_w, read_w, step_w, value_taps, write_taps, read_taps, past_values,
@@ -109,6 +110,10 @@
         wait(i)
         if place == len(order) - 1:
             start(17, 19, 20)
+            for d in range(n):
+                send1[d] = wide[d * seqs : (d + 1) * seqs, inner:].astype(BF16)
+            pl.semaphore_wait(barrier, n - 1)
+            first = exchange(lambda other: send1.at[other], lambda j: recv1.at[j], s1, r1)
         w = held[i]
         if i == 5:
             wide[:, offsets[4] : offsets[4] + HEADS] = lax.dot_general(
@@ -121,9 +126,8 @@
                 x[...], w[:, begin : begin + size], preferred_element_type=F32
             )
     for d in range(n):
-        send1[d] = wide[d * seqs : (d + 1) * seqs, :].astype(BF16)
-    pl.semaphore_wait(barrier, n - 1)
-    first = exchange(lambda other: send1.at[other], lambda j: recv1.at[j], s1, r1)
+        send_gate[d] = wide[d * seqs : (d + 1) * seqs, :inner].astype(BF16)
+    sixth = exchange(lambda other: send_gate.at[other], lambda j: recv_gate.at[j], s6, r6)
 
     wait(6, 7, 8, 9, 10, 11, 12, 13, 14, 16, 18, 21, 15)
     head_of = lax.broadcasted_iota(jnp.int32, (HEADS, inner), 1) // HEAD_DIM
@@ -144,11 +148,10 @@
         return silu(acc)
 
     groups = GROUPS * STATE_DIM
-    gate = total[:, offsets[0] : offsets[0] + inner]
-    values = conv(total[:, offsets[1] : offsets[1] + inner], past_values, value_taps)
-    writes = conv(total[:, offsets[2] : offsets[2] + groups], past_writes, write_taps)
-    reads = conv(total[:, offsets[3] : offsets[3] + groups], past_reads, read_taps)
-    raw = total[:, offsets[4] : offsets[4] + HEADS] + step_bias[...]
+    values = conv(total[:, offsets[1] - inner : offsets[1] - inner + inner], past_values, value_taps)
+    writes = conv(total[:, offsets[2] - inner : offsets[2] - inner + groups], past_writes, write_taps)
+    reads = conv(total[:, offsets[3] - inner : offsets[3] - inner + groups], past_reads, read_taps)
+    raw = total[:, offsets[4] - inner : offsets[4] - inner + HEADS] + step_bias[...]
     step_size = jnp.maximum(raw, 0.0) + jnp.log1p(jnp.exp(-jnp.abs(raw)))
     decays = jnp.exp(-step_size * jnp.exp(decay_log[...]))
     pad = spread.shape[0] // 3
@@ -179,7 +182,11 @@
     drive_out[0:seqs, :] = drive
     write_out[0:seqs, :] = writes
     base = decay_c * read_out[...] + skip_c * values
-    gate_act = silu(gate)
+    gate = send_gate[me].astype(F32)
+    for j in range(1, n):
+        sixth[j - 1].wait_recv()
+        gate = gate + recv_gate[j].astype(F32)
+    gate_act = silu(gate.astype(BF16).astype(F32))
     product = writes * reads
     for g in range(GROUPS):
         here = slice(g * half, (g + 1) * half)
@@ -221,12 +228,39 @@
     mix_out = jnp.dot(mix_rows[...].astype(BF16), out_w[...], preferred_element_type=F32)
     residual = RESIDUAL_SCALE * x[...].astype(F32) + mix_out.astype(BF16).astype(F32)
     res_all[me] = residual.astype(BF16)
-    third = exchange(lambda other: res_all.at[me], lambda j: res_all.at[me], s3, r3)
+    kv, tp = lax.axis_index("kv"), lax.axis_index("tp")
+    chips = n // tp_size
+
+    def to_device(block, send_sem, recv_sem, chip, core):
+        copy = pltpu.make_async_remote_copy(
+            src_ref=res_all.at[block],
+            dst_ref=res_all.at[block],
+            send_sem=send_sem,
+            recv_sem=recv_sem,
+            device_id={"kv": chip, "tp": core},
+            device_id_type=pl.DeviceIdType.MESH,
+        )
+        copy.start()
+        return copy
+
+    far = [
+        to_device(me, s3.at[j], r3.at[j], lax.rem(kv + j, chips), tp) for j in range(1, chips)
+    ]
+    near = [
+        to_device(me, s7.at[0, c], r7.at[0, c], kv, lax.rem(tp + c, tp_size))
+        for c in range(1, tp_size)
+    ]
     for g in range(1, GROUPS):
         update_states(g)
 
-    wait(19, 20)
-    for copy in third:
+    for j in range(1, chips):
+        far[j - 1].wait_recv()
+        block = lax.rem(kv + chips - j, chips) * tp_size + tp
+        near += [
+            to_device(block, s7.at[j, c], r7.at[j, c], kv, lax.rem(tp + c, tp_size))
+            for c in range(1, tp_size)
+        ]
+    for copy in near:
         copy.wait_recv()
     total1 = jnp.zeros((rows, 1), F32)
     for d in range(n):
@@ -248,7 +282,8 @@
         def _():
             own_normed[...] = normed_f[d * seqs : (d + 1) * seqs, :]
 
-    chunk = min(256, up_w.shape[1])
+    wait(19, 20)
+    chunk = min(512, up_w.shape[1])
 
     @pl.loop(0, up_w.shape[1] // chunk)
     def _(c):
@@ -307,9 +342,32 @@
     layer_out[...] = done_rows[...].astype(BF16)
     for store in stores:
         store.wait()
-    for group in [first, second, third, *fourth, fifth]:
+    for group in [first, sixth, second, far, near, *fourth, fifth]:
         for copy in group:
             copy.wait_send()
+
+
+def tail_kernel(rows_in, state_in, rows_out, state_out, rows_held, state_held, in_sem, out_sem):
+    seqs, depth = state_in.shape[0], state_in.shape[1] // 2
+    pieces = []
+    for s in range(seqs):
+        for part in range(2):
+            here = (s, pl.ds(part * depth, depth))
+            pieces.append((state_in.at[here], state_held.at[here], state_out.at[here]))
+    pieces.append((rows_in, rows_held, rows_out))
+    loads = [
+        pltpu.make_async_copy(src, mid, in_sem.at[i]) for i, (src, mid, _) in enumerate(pieces)
+    ]
+    stores = [
+        pltpu.make_async_copy(mid, dst, out_sem.at[i]) for i, (_, mid, dst) in enumerate(pieces)
+    ]
+    for copy in loads:
+        copy.start()
+    for load, store in zip(loads, stores):
+        load.wait()
+        store.start()
+    for copy in stores:
+        copy.wait()
 
 
 def on_device(n, tp_size, *args):
@@ -330,7 +388,8 @@
         args[i] = jnp.transpose(args[i], (1, 0, 2))
     for i in (12, 13, 14, 16, 18, 21):
         args[i] = args[i].reshape(1, -1)
-    ways, halves = 4, 2
+    ways, halves = 4, 4
+    chips = n // tp_size
     pad = (seqs + 7) // 8 * 8
     dma = pltpu.SemaphoreType.DMA
     scratch = [pltpu.VMEM(a.shape, a.dtype) for a in args]
@@ -339,8 +398,10 @@
         pltpu.VMEM((pad, inner), F32),
         pltpu.VMEM((pad, GROUPS * STATE_DIM), F32),
         pltpu.VMEM((rows, width), F32),
-        pltpu.VMEM((n, seqs, width), BF16),
-        pltpu.VMEM((n, seqs, width), BF16),
+        pltpu.VMEM((n, seqs, width - inner), BF16),
+        pltpu.VMEM((n, seqs, width - inner), BF16),
+        pltpu.VMEM((n, seqs, inner), BF16),
+        pltpu.VMEM((n, seqs, inner), BF16),
         pltpu.VMEM((3 * pad, HEADS), F32),
         pltpu.VMEM((seqs, inner), F32),
         pltpu.VMEM((n, seqs, inner), BF16),
@@ -359,7 +420,8 @@
         dma((20 + 2 * ways,)),
         dma((GROUPS,)),
         dma((n,)), dma((n,)), dma((n,)), dma((n,)), dma((n,)), dma((n,)),
-        dma((halves, n)), dma((halves, n)), dma((n,)), dma((n,)),
+        dma((halves, n)), dma((halves, n)), dma((n,)), dma((n,)), dma((n,)), dma((n,)),
+        dma((chips, tp_size)), dma((chips, tp_size)),
     ]
     geo = (n, tp_size, seqs, rows, width, tuple(offsets), ways, halves)
     result, state_next = pl.pallas_call(
@@ -376,6 +438,23 @@
         ),
         name="layer",
     )(*args)
+    result, state_next = pl.pallas_call(
+        tail_kernel,
+        out_shape=(
+            jax.ShapeDtypeStruct(result.shape, BF16),
+            jax.ShapeDtypeStruct(state_next.shape, F32),
+        ),
+        in_specs=[ANY] * 2,
+        out_specs=(ANY, ANY),
+        scratch_shapes=[
+            pltpu.VMEM(result.shape, BF16),
+            pltpu.VMEM(state_next.shape, F32),
+            dma((2 * seqs + 1,)),
+            dma((2 * seqs + 1,)),
+        ],
+        compiler_params=pltpu.CompilerParams(vmem_limit_bytes=67043328),
+        name="tail",
+    )(result, state_next)
     return result, state_next.reshape(state.shape)
 
 

time: 52.5 us -> 47.2 us (0.90)
  local copies, waits for them, and re-layouts: 6.16 us -> 0 us
  Pallas kernels: 45.5 us -> 46.4 us
    unnamed x2 -> x0, local copies, waits for them, and re-layouts: 6.16 us -> none
    pallas_call x0 -> x1, Pallas kernels: none -> 3.6 us  [on_device(): pl.pallas_call(tail_kernel, out_shape=(jax.ShapeDtypeStruct(result.shape,...]
    pallas_call x1, Pallas kernels: 45.5 us -> 42.8 us  [on_device(): pl.pallas_call(functools.partial(layer_kernel, geo), out_shape=(jax.Shape...]
where the time goes in v3:
time: 47.2 us; the launch traced here: 47.1 us
  Pallas kernels  46.4 us (98%)
  between operations  0.65 us (1%)
    pallas_call x1, Pallas kernels, on_device(): pl.pallas_call(functools.partial(layer_kernel, geo), out_shape=(jax.Shape...  42.8 us
    pallas_call x1, Pallas kernels, on_device(): pl.pallas_call(tail_kernel, out_shape=(jax.ShapeDtypeStruct(result.shape,...  3.6 us

profile of v3, /device:TPU:0, one launch (start us, length us, event | category | flops | bytes accessed | tf_op | source)
XLA Modules:
  0.0 47.1 jit_solution(7125196237093688117)
XLA Ops:
  0.6 42.8 %layer.1 = (bf16[32,512]{1,0:T(8,128)(2,1)}, f32[4,2048,128]{2,1,0:T(8,128)}) custom-call(bf16[32,512]{1,0:T(8,128)(2,1)} %refs_0_.1, bf16[512,2048]{1,0:T(8,128)(2,1)} %refs_1_.1, bf16[512,2048]{1,0:T(8,128)(2,1)} %refs_2_.1, bf16[512,256]{1,0:T(8,128)(2,1)} %refs_3_.1, bf16[512,256]{1,0:T(8,128)(2,1)} %refs_4_.1, bf16[32,512]{1,0:T(8,128)(2,1)} %bitcast.14, ...), custom_call_target="tpu_custom_call" | custom-call | tf_op jit(solution)/shard_map/layer/pallas_call | solution.py:427
  43.5 3.6 %tail.1 = (bf16[32,512]{1,0:T(8,128)(2,1)}, f32[4,2048,128]{2,1,0:T(8,128)}) custom-call(bf16[32,512]{1,0:T(8,128)(2,1)} %get-tuple-element.6.rows_in, f32[4,2048,128]{2,1,0:T(8,128)} %get-tuple-element.7.state_in), custom_call_target="tpu_custom_call" | custom-call | tf_op jit(solution)/shard_map/tail/pallas_call | solution.py:441
